TPU v7x, 32 devices: a whole 2x2x4 slice. The times are simulated.
32 devices in a mesh: sp: 16 (over z, y, x), tp: 2 (over core).
Axes of the slice: x: 2, y: 2, z: 4, core: 2. Of those that a mesh axis runs over, the one named last changes fastest.
Arguments:
- queries: bfloat16 [4096, 1024], P('sp', 'tp'), may hold values from -6 to 6
- keys: bfloat16 [4096, 256], P('sp'), may hold values from -6 to 6
- values: bfloat16 [4096, 256], P('sp'), may hold values from -6 to 6
- query_gain: float32 [128], replicated, may hold values from 1.4 to 5.5
- key_gain: float32 [128], replicated, may hold values from 1.4 to 5.5
- residual_in: bfloat16 [4096, 2048], P(('sp', 'tp')), may hold values from -6 to 6
- out_weight: bfloat16 [1024, 2048], P('tp'), may hold values from -0.1875 to 0.1875
- norm_gain: float32 [2048], replicated, may hold values from 0.1 to 1.9
- gate_weight: bfloat16 [2048, 3072], P('sp', 'tp'), may hold values from -0.125 to 0.125
- up_weight: bfloat16 [2048, 3072], P('sp', 'tp'), may hold values from -0.125 to 0.125
- down_weight: bfloat16 [3072, 2048], P('tp', 'sp'), may hold values from -0.109375 to 0.109375
Outputs:
- result: bfloat16 [4096, 2048], P(('sp', 'tp'))
All inputs are finite; a program needn't handle non-finite values.
Results may differ from a plain program's by a relative error of at most 0.017.
Values may be sent and summed in bfloat16 or wider, within the bound.
A program may use at most 64 MiB of HBM per device.

v0:
```python
import math
import jax
import jax.numpy as jnp
from jax import lax
from jax.sharding import PartitionSpec as P

Q_HEADS = 8
KV_HEADS = 2
GRID_WIDTH = 64
EPS = 1e-06
ROPE_BASE = 10000.0


def normalize(wide_values, gain):
    wide = wide_values.astype(jnp.float32)
    return wide * lax.rsqrt(jnp.mean(wide * wide, axis=-1, keepdims=True) + EPS) * gain


def rotate_pair(segment, angles):
    half_size = segment.shape[-1] // 2
    first = segment[..., :half_size]
    second = segment[..., half_size:]
    cosine = jnp.cos(angles)[:, None, :]
    sine_part = jnp.sin(angles)[:, None, :]
    return jnp.concatenate(
        [first * cosine - second * sine_part, second * cosine + first * sine_part], axis=-1
    )


def grid_rotary(head_rows, positions):
    head_size = head_rows.shape[-1]
    half_size = head_size // 2
    quarter = head_size // 4
    inverse = ROPE_BASE ** (-jnp.arange(quarter, dtype=jnp.float32) * 2.0 / half_size)
    row_angles = (positions // GRID_WIDTH).astype(jnp.float32)[:, None] * inverse
    col_angles = (positions % GRID_WIDTH).astype(jnp.float32)[:, None] * inverse
    return jnp.concatenate(
        [
            rotate_pair(head_rows[..., :half_size], row_angles),
            rotate_pair(head_rows[..., half_size:], col_angles),
        ],
        axis=-1,
    )


def gated(gate_part, lifted):
    return (jax.nn.silu(gate_part) * lifted).astype(jnp.bfloat16)


def local(
    queries,
    keys,
    values,
    query_gain,
    key_gain,
    residual_in,
    out_weight,
    norm_gain,
    gate_weight,
    up_weight,
    down_weight,
):
    tok_rows = queries.shape[0]
    head_size = query_gain.shape[0]
    local_heads = queries.shape[1] // head_size
    tp_index = lax.axis_index("tp")
    share = tok_rows // lax.axis_size("tp")
    positions = lax.axis_index("sp") * tok_rows + jnp.arange(tok_rows, dtype=jnp.int32)
    key_head = tp_index * local_heads // (Q_HEADS // KV_HEADS)
    own_keys = lax.dynamic_slice_in_dim(keys, key_head * head_size, head_size, 1)
    own_values = lax.dynamic_slice_in_dim(values, key_head * head_size, head_size, 1)
    turned_keys = grid_rotary(
        normalize(own_keys.reshape(tok_rows, 1, head_size), key_gain), positions
    )
    turned_keys = turned_keys.reshape(tok_rows, head_size).astype(jnp.bfloat16)
    turned_queries = grid_rotary(
        normalize(queries.reshape(tok_rows, local_heads, head_size), query_gain), positions
    )
    turned_queries = turned_queries.reshape(tok_rows * local_heads, head_size).astype(jnp.bfloat16)
    score_scale = head_size ** (-0.5)

    def attend_block(running, block_pair):
        peak_score, weight_total, weighted = running
        block_keys, block_values = block_pair
        scores = (
            lax.dot_general(
                turned_queries,
                block_keys,
                (((1,), (1,)), ((), ())),
                preferred_element_type=jnp.float32,
            )
            * score_scale
        )
        new_peak = jnp.maximum(peak_score, jnp.max(scores, axis=1))
        factor = jnp.exp(peak_score - new_peak)
        raw = jnp.exp(scores - new_peak[:, None])
        weight_total = weight_total * factor + jnp.sum(raw, axis=1)
        weighted = weighted * factor[:, None] + jnp.dot(
            raw.astype(jnp.bfloat16), block_values, preferred_element_type=jnp.float32
        )
        return ((new_peak, weight_total, weighted), None)

    row_count = tok_rows * local_heads
    start_carry = (
        jnp.full((row_count,), -1e30, jnp.float32),
        jnp.zeros((row_count,), jnp.float32),
        jnp.zeros((row_count, head_size), jnp.float32),
    )
    piece_keys = lax.all_gather(turned_keys, "sp", axis=0, tiled=True)
    piece_values = lax.all_gather(own_values, "sp", axis=0, tiled=True)
    span = math.gcd(piece_keys.shape[0], 512)
    blocks = piece_keys.shape[0] // span
    stacked = (
        piece_keys.reshape(blocks, span, head_size),
        piece_values.reshape(blocks, span, head_size),
    )
    updated, unused = lax.scan(attend_block, start_carry, stacked)
    peak_score, weight_total, weighted = updated
    attended = (
        (weighted / weight_total[:, None])
        .astype(jnp.bfloat16)
        .reshape(tok_rows, local_heads * head_size)
    )
    placed = lax.dynamic_update_slice_in_dim(
        jnp.zeros((tok_rows, residual_in.shape[1]), jnp.float32),
        residual_in.astype(jnp.float32),
        tp_index * share,
        0,
    )
    head_partial = jnp.dot(attended, out_weight, preferred_element_type=jnp.float32)
    partial_total, residual_rows = (
        lax.psum(head_partial.astype(jnp.bfloat16), "tp").astype(jnp.float32),
        lax.psum(placed.astype(jnp.bfloat16), "tp").astype(jnp.float32),
    )
    middle_rows = (residual_rows + partial_total).astype(jnp.bfloat16)
    normed = normalize(middle_rows, norm_gain).astype(jnp.bfloat16)
    middle = lax.dynamic_slice_in_dim(middle_rows, tp_index * share, share, 0)
    hidden_width = gate_weight.shape[1]
    side_by_side = jnp.concatenate(
        [
            lax.all_gather(gate_weight, "sp", axis=0, tiled=True),
            lax.all_gather(up_weight, "sp", axis=0, tiled=True),
        ],
        axis=1,
    )
    both_parts = jnp.dot(normed, side_by_side, preferred_element_type=jnp.float32)
    hidden = gated(both_parts[:, :hidden_width], both_parts[:, hidden_width:])
    partials = jnp.dot(
        hidden,
        lax.all_gather(down_weight, "sp", axis=1, tiled=True),
        preferred_element_type=jnp.float32,
    )
    mixer_out = lax.psum_scatter(
        partials.astype(jnp.bfloat16), "tp", scatter_dimension=0, tiled=True
    ).astype(jnp.float32)
    return (middle.astype(jnp.float32) + mixer_out).astype(jnp.bfloat16)


def solution(mesh):
    return jax.shard_map(
        local,
        mesh=mesh,
        in_specs=(
            P("sp", "tp"),
            P("sp", None),
            P("sp", None),
            P(),
            P(),
            P(("sp", "tp"), None),
            P("tp", None),
            P(),
            P("sp", "tp"),
            P("sp", "tp"),
            P("tp", "sp"),
        ),
        out_specs=P(("sp", "tp"), None),
        check_vma=False,
    )
```

profile of v0, /device:TPU:0, one launch (start us, length us, event | category | flops | bytes accessed | tf_op | source)
XLA Modules:
  0.0 528.7 jit_solution(11063251506600256293)
XLA Ops:
  6.6 1.0 constant_dynamic-slice_fusion.1
  7.7 0.7 fusion.29
  8.8 0.6 pad_maximum_fusion.1
  9.5 1.5 constant_dynamic-slice_fusion
  11.1 1.1 reshape.287
  12.6 1.0 multiply_cosine_fusion.1
  13.9 0.9 subtract_convert_fusion.1
  14.9 0.8 pad_maximum_fusion
  15.7 1.1 broadcast_in_dim.8
  16.8 0.9 convert_dynamic-update-slice_fusion
  17.7 50.1 %all-gather.15.cloned.1.call-done = bf16[4096,1,128]{0,2,1:T(8,128)(2,1)} async-done(((bf16[256,1,128]{0,2,1:T(8,128)(2,1)}), bf16[4096,1,128]{0,2,1:T(8,128)(2,1)}) %all-gather.15.cloned.1.call-update) | async-done | bytes 1048592 | tf_op jit(solution)/shard_map/all_gather | solution.py:109
  67.8 2.3 copy.19
  70.1 54.3 %all-gather.7.cloned.1.call-done = bf16[4096,128]{1,0:T(8,128)(2,1)} async-done(((bf16[256,128]{1,0:T(8,128)(2,1)}), bf16[4096,128]{1,0:T(8,128)(2,1)}) %all-gather.7.cloned.1.call-update) | async-done | bytes 1048592 | tf_op jit(solution)/shard_map/all_gather | solution.py:110
  124.4 51.7 %while.15 = (s32[]{:T(128)}, f32[1024]{0:T(1024)S(1)}, f32[1024]{0:T(1024)S(1)}, f32[1024,128]{1,0:T(8,128)S(1)}, bf16[8,512,128]{2,1,0:T(8,128)(2,1)}, /*index=...) while((s32[]{:T(128)}, f32[1024]{0:T(1024)S(1)}, ...), condition=%wide.region_6.7_spmd.clone, body=%wide.region_3.6_spmd.clone.sunk | while | flops 273028096 | bytes 16319621 | solution.py:117
  124.4 2.7 multiply_reduce_fusion.3
  127.0 2.1 fusion.63
  129.3 1.5 convolution_add_fusion.2
  130.8 2.7 multiply_reduce_fusion.3
  133.5 2.1 fusion.63
  135.7 1.5 convolution_add_fusion.2
  137.3 2.7 multiply_reduce_fusion.3
  140.0 2.1 fusion.63
  142.2 1.5 convolution_add_fusion.2
  143.7 2.7 multiply_reduce_fusion.3
  146.4 2.1 fusion.63
  148.6 1.5 convolution_add_fusion.2
  150.2 2.7 multiply_reduce_fusion.3
  152.9 2.1 fusion.63
  155.1 1.5 convolution_add_fusion.2
  156.7 2.7 multiply_reduce_fusion.3
  159.3 2.1 fusion.63
  161.6 1.5 convolution_add_fusion.2
  163.1 2.7 multiply_reduce_fusion.3
  165.8 2.1 fusion.63
  168.0 1.5 convolution_add_fusion.2
  169.6 2.7 multiply_reduce_fusion.3
  172.3 2.1 fusion.63
  174.5 1.5 convolution_add_fusion.2
  176.4 1.7 convolution_convert_fusion
  179.9 18.6 %all-reduce.3.cloned.1.call-done = (bf16[256,2048]{1,0:T(8,128)(2,1)}, bf16[256,2048]{1,0:T(8,128)(2,1)}) async-done(((bf16[256,2048]{1,0:T(8,128)(2,1)}, bf16[256,2048]{1,0:T(8,128)(2,1)}), (bf16[256,2048]{1,0:T(8,128)(2,1)}, bf16[256,2048]{1,0:T(8,128)(2,1)})) %all-reduce.3.cloned.1.call-update) | async-done | bytes 2097168 | tf_op jit(solution)/shard_map/psum | solution.py:132
  198.5 2.0 fusion.18
  200.6 95.2 %all-gather.11.cloned.1.call-done = bf16[2048,1536]{1,0:T(8,128)(2,1)} async-done(((bf16[128,1536]{1,0:T(8,128)(2,1)}), bf16[2048,1536]{1,0:T(8,128)(2,1)}) %all-gather.11.cloned.1.call-update) | async-done | bytes 6291472 | tf_op jit(solution)/shard_map/all_gather | solution.py:142
  295.8 94.6 %all-gather.9.cloned.1.call-done = bf16[2048,1536]{1,0:T(8,128)(2,1)} async-done(((bf16[128,1536]{1,0:T(8,128)(2,1)}), bf16[2048,1536]{1,0:T(8,128)(2,1)}) %all-gather.9.cloned.1.call-update) | async-done | bytes 6291472 | tf_op jit(solution)/shard_map/all_gather | solution.py:141
  390.4 9.8 %fusion.14 = f32[256,3072]{1,0:T(8,128)} fusion(bf16[2048,1536]{1,0:T(8,128)(2,1)} %all-gather.11.cloned.1.call-done, bf16[2048,1536]{1,0:T(8,128)(2,1)} %all-gather.9.cloned.1.call-done, bf16[256,2048]{1,0:T(8,128)(2,1)S(1)} %get-tuple-element.102, f32[2048]{0:T(1024)S(1)} %copy-done.4, f32[256]{0:T(256)S(1)} %add_rsqrt_fusion.1), kind=kOutput, calls=%fused_computation.20 | convolution fusion | flops 3248488448 | bytes 16786432 | tf_op jit(solution)/shard_map/dot_general | solution.py:146
  400.2 106.3 %all-gather.13.cloned.1.call-done = bf16[1536,2048]{1,0:T(8,128)(2,1)} async-done(((bf16[1536,128]{1,0:T(8,128)(2,1)}), bf16[1536,2048]{1,0:T(8,128)(2,1)}) %all-gather.13.cloned.1.call-update) | async-done | bytes 6291472 | tf_op jit(solution)/shard_map/all_gather | solution.py:150
  506.5 6.6 %convolution_convert_fusion.1 = bf16[256,2048]{1,0:T(8,128)(2,1)} fusion(bf16[1536,2048]{1,0:T(8,128)(2,1)} %all-gather.13.cloned.1.call-done, f32[256,3072]{1,0:T(8,128)} %fusion.14), kind=kOutput, calls=%fused_computation.27 | convolution fusion | flops 1613496320 | bytes 10485760 | tf_op jit(solution)/shard_map/dot_general | solution.py:148
  513.1 6.7 %reduce-scatter.2.cloned.1.call-done = bf16[128,2048]{1,0:T(8,128)(2,1)} async-done(((bf16[256,2048]{1,0:T(8,128)(2,1)}), bf16[128,2048]{1,0:T(8,128)(2,1)}) %reduce-scatter.2.cloned.1.call-update) | async-done | bytes 524304 | tf_op jit(solution)/shard_map/reduce_scatter | solution.py:153
  519.9 2.0 add_convert_fusion.1
  (77 shorter events, 4.4 us)
Async XLA Ops:
  6.5 169.9 %copy-start = (bf16[512,2048]{1,0:T(8,128)(2,1)S(1)}, bf16[512,2048]{1,0:T(8,128)(2,1)}, u32[]{:S(2)}) copy-start(bf16[512,2048]{1,0:T(8,128)(2,1)} %param.19) | copy-start | bytes 6291460
  6.5 7.1 %copy-start.3 = (f32[128]{0:T(128)S(1)}, f32[128]{0:T(128)}, u32[]{:S(2)}) copy-start(f32[128]{0:T(128)} %param.16) | copy-start | bytes 1540
  6.5 61.3 %all-gather.15.cloned.1.call-start = ((), (), s32[]{:S(2)}) async-start(), calls=%async_computation.6 | async-start | bytes 1114112 | tf_op jit(solution)/shard_map/all_gather | solution.py:109
  9.5 114.9 %all-gather.7.cloned.1.call-start = ((), (), s32[]{:S(2)}) async-start(), calls=%async_computation.1 | async-start | bytes 1114112 | tf_op jit(solution)/shard_map/all_gather | solution.py:110
  11.0 187.5 %all-reduce.3.cloned.1.call-start = ((), (), s32[]{:S(2)}) async-start(), calls=%async_computation.7 | async-start | bytes 4194304 | tf_op jit(solution)/shard_map/psum | solution.py:132
  14.8 2.0 copy-start.2
  127.0 2.2 copy-start.1
  133.5 2.2 copy-start.1
  140.0 2.2 copy-start.1
  146.4 2.2 copy-start.1
  152.9 2.2 copy-start.1
  159.3 2.2 copy-start.1
  165.8 2.2 copy-start.1
  172.3 2.2 copy-start.1
  178.1 212.2 %copy-start.4 = (f32[2048]{0:T(1024)S(1)}, f32[2048]{0:T(1024)}, u32[]{:S(2)}) copy-start(f32[2048]{0:T(1024)} %param.20) | copy-start | bytes 24580
  178.1 117.6 %all-gather.11.cloned.1.call-start = ((), (), s32[]{:S(2)}) async-start(), calls=%async_computation.3 | async-start | bytes 6684672 | tf_op jit(solution)/shard_map/all_gather | solution.py:142
  178.7 211.6 %all-gather.9.cloned.1.call-start = ((), (), s32[]{:S(2)}) async-start(), calls=%async_computation.2 | async-start | bytes 6684672 | tf_op jit(solution)/shard_map/all_gather | solution.py:141
  179.3 327.2 %all-gather.13.cloned.1.call-start = ((), (), s32[]{:S(2)}) async-start(), calls=%async_computation.4 | async-start | bytes 6684672 | tf_op jit(solution)/shard_map/all_gather | solution.py:150
  179.9 340.0 %reduce-scatter.2.cloned.1.call-start = ((), (), s32[]{:S(2)}) async-start(), calls=%async_computation.5 | async-start | bytes 1572864 | tf_op jit(solution)/shard_map/reduce_scatter | solution.py:153
Sparse Core Ops, SparseCore 0:
  10.1 57.6 all-gather.14
  70.6 53.7 all-gather.6
  178.3 20.2 all-reduce.2
  201.1 94.5 all-gather.10
  298.4 91.9 all-gather.8
  392.9 113.5 all-gather.12
  513.2 6.5 reduce-scatter.1
where the time goes:
time: 529 us
  waiting for transfers between devices  428 us (81%)
  matrix products  51.7 us (10%)
  other arithmetic  27.3 us (5%)
  between operations  13.7 us (3%)
  local copies, waits for them, and re-layouts  8.01 us (2%)
    all_gather x1, waiting for transfers between devices, local(): lax.all_gather(down_weight, 'sp', axis=1, tiled=True)  106 us
    all_gather x1, waiting for transfers between devices, local(): lax.all_gather(up_weight, 'sp', axis=0, tiled=True)  95.2 us
    all_gather x1, waiting for transfers between devices, local(): lax.all_gather(gate_weight, 'sp', axis=0, tiled=True)  94.6 us
    all_gather x1, waiting for transfers between devices, local(): piece_values = lax.all_gather(own_values, 'sp', axis=0, tiled=True)  54.3 us
    all_gather x1, waiting for transfers between devices, local(): piece_keys = lax.all_gather(turned_keys, 'sp', axis=0, tiled=True)  50.1 us
    dot_general x8, matrix products, attend_block(): lax.dot_general(turned_queries, block_keys, (((1,), (1,)), ((), ())), pre...  21.4 us
    psum x1, waiting for transfers between devices, local(): lax.psum(head_partial.astype(jnp.bfloat16), 'tp').astype(jnp.float32)  18.6 us
    reduce_sum x8, other arithmetic, attend_block(): weight_total = weight_total * factor + jnp.sum(raw, axis=1)  16.9 us
  transfers between devices with their start and end apart: 7, of which 7 were waited for; matrix products, arithmetic and copies ran while one was open for 4% of the time, Pallas kernels for 0%

commit v1 on v0

--- a/solution.py
+++ b/solution.py
@@ -147,7 +147,7 @@
     hidden = gated(both_parts[:, :hidden_width], both_parts[:, hidden_width:])
     partials = jnp.dot(
         hidden,
-        lax.all_gather(down_weight, "sp", axis=1, tiled=True),
+        jnp.concatenate(lax.all_gather(down_weight, "sp"), axis=1),
         preferred_element_type=jnp.float32,
     )
     mixer_out = lax.psum_scatter(

time: 529 us -> 513 us (0.970)
  waiting for transfers between devices: 428 us -> 407 us
  local copies, waits for them, and re-layouts: 8.01 us -> 16.8 us
  matrix products: 51.7 us -> 46.4 us
    all_gather x1, waiting for transfers between devices: 106 us -> 95.2 us  [local(): lax.all_gather(down_weight, 'sp')]
    all_gather x1, waiting for transfers between devices: 94.6 us -> 85.8 us  [local(): lax.all_gather(gate_weight, 'sp', axis=0, tiled=True)]
    reshape x0 -> x1, local copies, waits for them, and re-layouts: none -> 8.76 us  [local(): jnp.concatenate(lax.all_gather(down_weight, 'sp'), axis=1)]
where the time goes in v1:
time: 513 us; the launch traced here: 512 us
  waiting for transfers between devices  407 us (79%)
  matrix products  46.4 us (9%)
  other arithmetic  27.3 us (5%)
  local copies, waits for them, and re-layouts  16.8 us (3%)
  between operations  13.7 us (3%)
    all_gather x1, waiting for transfers between devices, local(): lax.all_gather(down_weight, 'sp')  95.2 us
    all_gather x1, waiting for transfers between devices, local(): lax.all_gather(up_weight, 'sp', axis=0, tiled=True)  94.6 us
    all_gather x1, waiting for transfers between devices, local(): lax.all_gather(gate_weight, 'sp', axis=0, tiled=True)  85.8 us
    all_gather x1, waiting for transfers between devices, local(): piece_values = lax.all_gather(own_values, 'sp', axis=0, tiled=True)  54.3 us
    all_gather x1, waiting for transfers between devices, local(): piece_keys = lax.all_gather(turned_keys, 'sp', axis=0, tiled=True)  50.1 us
    dot_general x8, matrix products, attend_block(): lax.dot_general(turned_queries, block_keys, (((1,), (1,)), ((), ())), pre...  21.4 us
    psum x1, waiting for transfers between devices, local(): lax.psum(head_partial.astype(jnp.bfloat16), 'tp').astype(jnp.float32)  18.4 us
    reduce_sum x8, other arithmetic, attend_block(): weight_total = weight_total * factor + jnp.sum(raw, axis=1)  16.9 us
  transfers between devices with their start and end apart: 7, of which 7 were waited for; matrix products, arithmetic and copies ran while one was open for 4% of the time, Pallas kernels for 0%

profile of v1, /device:TPU:0, one launch (start us, length us, event | category | flops | bytes accessed | tf_op | source)
XLA Modules:
  0.0 511.9 jit_solution(1291841046959933060)
XLA Ops:
  6.6 1.0 constant_dynamic-slice_fusion.1
  7.7 0.7 fusion.29
  9.5 1.5 constant_dynamic-slice_fusion
  11.1 1.1 reshape.295
  12.6 1.0 multiply_cosine_fusion.1
  14.0 0.9 subtract_convert_fusion.1
  14.9 0.8 pad_maximum_fusion
  15.7 1.1 broadcast_in_dim.8
  16.8 0.9 convert_dynamic-update-slice_fusion
  17.7 50.1 %all-gather.14.cloned.1.call-done = bf16[4096,1,128]{0,2,1:T(8,128)(2,1)} async-done(((bf16[256,1,128]{0,2,1:T(8,128)(2,1)}), bf16[4096,1,128]{0,2,1:T(8,128)(2,1)}) %all-gather.14.cloned.1.call-update) | async-done | bytes 1048592 | tf_op jit(solution)/shard_map/all_gather | solution.py:109
  67.8 2.3 copy.22
  70.1 54.3 %all-gather.8.cloned.1.call-done = bf16[4096,128]{1,0:T(8,128)(2,1)} async-done(((bf16[256,128]{1,0:T(8,128)(2,1)}), bf16[4096,128]{1,0:T(8,128)(2,1)}) %all-gather.8.cloned.1.call-update) | async-done | bytes 1048592 | tf_op jit(solution)/shard_map/all_gather | solution.py:110
  124.4 51.6 %while.15 = (s32[]{:T(128)}, f32[1024]{0:T(1024)S(1)}, f32[1024]{0:T(1024)S(1)}, f32[1024,128]{1,0:T(8,128)S(1)}, bf16[8,512,128]{2,1,0:T(8,128)(2,1)}, /*index=...) while((s32[]{:T(128)}, f32[1024]{0:T(1024)S(1)}, ...), condition=%wide.region_6.7_spmd.clone, body=%wide.region_3.6_spmd.clone.sunk | while | flops 273028096 | bytes 16319621 | solution.py:117
  124.4 2.7 multiply_reduce_fusion.3
  127.0 2.1 fusion.63
  129.3 1.5 convolution_add_fusion.2
  130.8 2.7 multiply_reduce_fusion.3
  133.5 2.1 fusion.63
  135.7 1.5 convolution_add_fusion.2
  137.3 2.7 multiply_reduce_fusion.3
  140.0 2.1 fusion.63
  142.2 1.5 convolution_add_fusion.2
  143.7 2.7 multiply_reduce_fusion.3
  146.4 2.1 fusion.63
  148.6 1.5 convolution_add_fusion.2
  150.2 2.7 multiply_reduce_fusion.3
  152.9 2.1 fusion.63
  155.1 1.5 convolution_add_fusion.2
  156.6 2.7 multiply_reduce_fusion.3
  159.3 2.1 fusion.63
  161.5 1.5 convolution_add_fusion.2
  163.1 2.7 multiply_reduce_fusion.3
  165.8 2.1 fusion.63
  168.0 1.5 convolution_add_fusion.2
  169.5 2.7 multiply_reduce_fusion.3
  172.2 2.1 fusion.63
  174.4 1.5 convolution_add_fusion.2
  176.4 1.7 convolution_convert_fusion
  180.1 18.4 %all-reduce.3.cloned.1.call-done = (bf16[256,2048]{1,0:T(8,128)(2,1)}, bf16[256,2048]{1,0:T(8,128)(2,1)}) async-done(((bf16[256,2048]{1,0:T(8,128)(2,1)}, bf16[256,2048]{1,0:T(8,128)(2,1)}), (bf16[256,2048]{1,0:T(8,128)(2,1)}, bf16[256,2048]{1,0:T(8,128)(2,1)})) %all-reduce.3.cloned.1.call-update) | async-done | bytes 2097168 | tf_op jit(solution)/shard_map/psum | solution.py:132
  198.5 2.0 fusion.18
  200.6 95.2 %all-gather.16.cloned.1.call-done = bf16[24576,128]{1,0:T(8,128)(2,1)} async-done(((bf16[1536,128]{1,0:T(8,128)(2,1)}), bf16[24576,128]{1,0:T(8,128)(2,1)}) %all-gather.16.cloned.1.call-update) | async-done | bytes 6291472 | tf_op jit(solution)/shard_map/all_gather | solution.py:150
  295.7 8.8 %copy.21 = bf16[1536,16,128]{0,2,1:T(8,128)(2,1)} copy(bf16[1536,16,128]{2,0,1:T(8,128)(2,1)} %bitcast.28) | data formatting | bytes 12582912 | tf_op jit(solution)/shard_map/reshape | solution.py:150
  304.5 85.8 %all-gather.10.cloned.1.call-done = bf16[2048,1536]{1,0:T(8,128)(2,1)} async-done(((bf16[128,1536]{1,0:T(8,128)(2,1)}), bf16[2048,1536]{1,0:T(8,128)(2,1)}) %all-gather.10.cloned.1.call-update) | async-done | bytes 6291472 | tf_op jit(solution)/shard_map/all_gather | solution.py:141
  390.3 94.6 %all-gather.12.cloned.1.call-done = bf16[2048,1536]{1,0:T(8,128)(2,1)} async-done(((bf16[128,1536]{1,0:T(8,128)(2,1)}), bf16[2048,1536]{1,0:T(8,128)(2,1)}) %all-gather.12.cloned.1.call-update) | async-done | bytes 6291472 | tf_op jit(solution)/shard_map/all_gather | solution.py:142
  484.9 8.3 %fusion.14 = f32[256,3072]{1,0:T(8,128)S(1)} fusion(bf16[2048,1536]{1,0:T(8,128)(2,1)} %all-gather.12.cloned.1.call-done, bf16[2048,1536]{1,0:T(8,128)(2,1)} %all-gather.10.cloned.1.call-done, bf16[256,2048]{1,0:T(8,128)(2,1)S(1)} %get-tuple-element.102, f32[2048]{0:T(1024)S(1)} %copy-done.5, f32[256]{0:T(256)S(1)} %add_rsqrt_fusion.1), kind=kOutput, calls=%fused_computation.20 | convolution fusion | flops 3248488448 | bytes 16786432 | tf_op jit(solution)/shard_map/dot_general | solution.py:146
  493.2 2.8 convolution_convert_fusion.1
  496.0 7.1 %reduce-scatter.2.cloned.1.call-done = bf16[128,2048]{1,0:T(8,128)(2,1)} async-done(((bf16[256,2048]{1,0:T(8,128)(2,1)}), bf16[128,2048]{1,0:T(8,128)(2,1)}) %reduce-scatter.2.cloned.1.call-update) | async-done | bytes 524304 | tf_op jit(solution)/shard_map/reduce_scatter | solution.py:153
  503.1 2.0 add_convert_fusion.1
  (80 shorter events, 5.2 us)
Async XLA Ops:
  6.5 169.8 %copy-start = (bf16[512,2048]{1,0:T(8,128)(2,1)S(1)}, bf16[512,2048]{1,0:T(8,128)(2,1)}, u32[]{:S(2)}) copy-start(bf16[512,2048]{1,0:T(8,128)(2,1)} %param.19) | copy-start | bytes 6291460
  6.5 7.1 %copy-start.4 = (f32[128]{0:T(128)S(1)}, f32[128]{0:T(128)}, u32[]{:S(2)}) copy-start(f32[128]{0:T(128)} %param.16) | copy-start | bytes 1540
  6.5 61.3 %all-gather.14.cloned.1.call-start = ((), (), s32[]{:S(2)}) async-start(), calls=%async_computation.5 | async-start | bytes 1114112 | tf_op jit(solution)/shard_map/all_gather | solution.py:109
  9.5 114.9 %all-gather.8.cloned.1.call-start = ((), (), s32[]{:S(2)}) async-start(), calls=%async_computation.1 | async-start | bytes 1114112 | tf_op jit(solution)/shard_map/all_gather | solution.py:110
  11.0 187.5 %all-reduce.3.cloned.1.call-start = ((), (), s32[]{:S(2)}) async-start(), calls=%async_computation.7 | async-start | bytes 4194304 | tf_op jit(solution)/shard_map/psum | solution.py:132
  14.9 2.0 copy-start.3
  127.0 2.2 copy-start.1
  133.5 2.2 copy-start.1
  139.9 2.2 copy-start.1
  146.4 2.2 copy-start.1
  152.9 2.2 copy-start.1
  159.3 2.2 copy-start.1
  165.8 2.2 copy-start.1
  172.2 2.2 copy-start.1
  178.1 117.6 %all-gather.16.cloned.1.call-start = ((), (), s32[]{:S(2)}) async-start(), calls=%async_computation.6 | async-start | bytes 6684672 | tf_op jit(solution)/shard_map/all_gather | solution.py:150
  178.7 211.6 %all-gather.10.cloned.1.call-start = ((), (), s32[]{:S(2)}) async-start(), calls=%async_computation.2 | async-start | bytes 6684672 | tf_op jit(solution)/shard_map/all_gather | solution.py:141
  179.3 305.6 %all-gather.12.cloned.1.call-start = ((), (), s32[]{:S(2)}) async-start(), calls=%async_computation.3 | async-start | bytes 6684672 | tf_op jit(solution)/shard_map/all_gather | solution.py:142
  179.9 323.3 %reduce-scatter.2.cloned.1.call-start = ((), (), s32[]{:S(2)}) async-start(), calls=%async_computation.4 | async-start | bytes 1572864 | tf_op jit(solution)/shard_map/reduce_scatter | solution.py:153
  295.7 189.2 %copy-start.5 = (f32[2048]{0:T(1024)S(1)}, f32[2048]{0:T(1024)}, u32[]{:S(2)}) copy-start(f32[2048]{0:T(1024)} %param.20) | copy-start | bytes 24580
  484.9 8.3 %copy-start.2 = (bf16[1536,16,128]{0,2,1:T(8,128)(2,1)S(1)}, bf16[1536,16,128]{0,2,1:T(8,128)(2,1)}, u32[]{:S(2)}) copy-start(bf16[1536,16,128]{0,2,1:T(8,128)(2,1)} %copy.21) | copy-start | bytes 18874372
Sparse Core Ops, SparseCore 0:
  10.1 57.6 all-gather.13
  70.6 53.7 all-gather.7
  178.2 20.2 all-reduce.2
  201.1 94.5 all-gather.15
  298.4 91.9 all-gather.9
  393.0 91.9 all-gather.11
  496.2 6.8 reduce-scatter.1
